TPU v7x, 128 devices: a whole 4x4x4 slice. The times are simulated.
128 devices in a mesh: rep: 2 (over z_hi), fs: 32 (over z_lo, y, x), tp: 2 (over core).
Axes of the slice: x: 4, y: 4, z: 4 (z_hi: 2, z_lo: 2; z = z_hi * 2 + z_lo), core: 2. Of those that a mesh axis runs over, the one named last changes fastest.
Arguments:
- tokens: bfloat16 [64, 1024, 2048], P(('rep', 'fs'), 'tp'), may hold values from -6 to 6
- mix_gain: float32 [2048], replicated, may hold values from 0.1 to 1.9
- out_gate_w: float32 [2048, 1024], P('fs', 'tp'), may hold values from -0.125 to 0.125
- in_gate_w: float32 [2048, 1024], P('fs', 'tp'), may hold values from -0.125 to 0.125
- value_w: float32 [2048, 1024], P('fs', 'tp'), may hold values from -0.125 to 0.125
- out_gate_scale: float32 [1024], P(('tp', 'fs')), may hold values from 0.28 to 3.5
- in_gate_scale: float32 [1024], P(('tp', 'fs')), may hold values from 0.5 to 2
- value_scale: float32 [1024], P(('tp', 'fs')), may hold values from 0.5 to 2
- mix_taps: float32 [3, 1024], P(None, 'tp'), may hold values from -3.5 to 3.5
- conv_gain: float32 [1024], P('tp'), may hold values from 0.1 to 1.9
- out_proj_w: float32 [1024, 2048], P('tp', 'fs'), may hold values from -0.1875 to 0.1875
- proj_scale: float32 [2048], P('fs'), may hold values from 0.5 to 2
- ffn_gain: float32 [2048], replicated, may hold values from 0.1 to 1.9
- gate_w: float32 [2048, 2816], P('fs', 'tp'), may hold values from -0.125 to 0.125
- up_w: float32 [2048, 2816], P('fs', 'tp'), may hold values from -0.125 to 0.125
- gate_scale: float32 [2816], P(('tp', 'fs')), may hold values from 0.5 to 2
- up_scale: float32 [2816], P(('tp', 'fs')), may hold values from 0.5 to 2
- gate_taps: float32 [3, 2816], P(None, 'tp'), may hold values from -3.5 to 3.5
- up_taps: float32 [3, 2816], P(None, 'tp'), may hold values from -3.5 to 3.5
- gate_bias: float32 [2816], P('tp'), may hold values from -3 to 3
- up_bias: float32 [2816], P('tp'), may hold values from -3 to 3
- down_w: float32 [2816, 2048], P('tp', 'fs'), may hold values from -0.109375 to 0.109375
- down_scale: float32 [2048], P('fs'), may hold values from 0.5 to 2
Outputs:
- layer_out: bfloat16 [64, 1024, 2048], P(('rep', 'fs'), 'tp')
All inputs are finite; a program needn't handle non-finite values.
Results may differ from a plain program's by a relative error of at most 0.02.
Values may be sent and summed in bfloat16 or wider, within the bound.
A program may use at most 128 MiB of HBM per device.

v0:
```python
import jax
import jax.numpy as jnp
from jax import lax
from jax.sharding import PartitionSpec as P

epsilon = 1e-06


def joined_along(parts, dim):
    shape = list(parts.shape[1:])
    shape[dim] *= parts.shape[0]
    return jnp.moveaxis(parts, 0, dim).reshape(shape)


def gather_packed(arrays, axis, dims):
    ravelled = jnp.concatenate([a.reshape(-1) for a in arrays])
    lines, at, done = (lax.all_gather(ravelled, axis), 0, [])
    for a, dim in zip(arrays, dims):
        parts = lines[:, at : at + a.size].reshape(-1, *a.shape)
        done.append(joined_along(parts, dim))
        at += a.size
    return tuple(done)


def side_by_side(arrays, axis, dim, along):
    widths = [a.shape[along] for a in arrays]
    both = jnp.concatenate(arrays, axis=along)
    filled = lax.all_gather(both, axis, axis=dim, tiled=True)
    return tuple(jnp.split(filled, [sum(widths[:k]) for k in range(1, len(widths))], axis=along))


def from_everyone(shard, axis):
    size = lax.axis_size(axis)
    return lax.all_to_all(
        jnp.broadcast_to(shard[None], (size, *shard.shape)), axis, 0, 0, tiled=True
    )


def of_everyone(shard, axis):
    return from_everyone(shard, axis).sum(axis=0)


def collect(shard, axis, dim):
    return joined_along(from_everyone(shard, axis), dim)


def split_up(shard, dim, size):
    before, after = (shard.shape[:dim], shard.shape[dim + 1 :])
    return jnp.moveaxis(shard.reshape(*before, size, -1, *after), dim, 0)


def summed_on_arrival(shard, axis, dim):
    size = lax.axis_size(axis)
    parts = lax.all_to_all(split_up(shard, dim, size), axis, 0, 0, tiled=True)
    return jnp.sum(parts.astype(jnp.float32), axis=0)


def norm_rows(values, gain):
    return values * lax.rsqrt(jnp.mean(values * values, axis=-1, keepdims=True) + epsilon) * gain


def causal_taps(values, taps):
    kernel = taps.shape[0]
    length = values.shape[0]
    padded = jnp.pad(values, ((kernel - 1, 0), (0, 0)))
    total = jnp.zeros(values.shape, jnp.float32)
    for offset in range(kernel):
        total = total + taps[offset] * padded[offset : offset + length]
    return total


def column_block(left, scale_all, piece):
    return jnp.dot(left, piece, preferred_element_type=jnp.float32) * scale_all


def local(
    tokens,
    mix_gain,
    out_gate_w,
    in_gate_w,
    value_w,
    out_gate_scale,
    in_gate_scale,
    value_scale,
    mix_taps,
    conv_gain,
    out_proj_w,
    proj_scale,
    ffn_gain,
    gate_w,
    up_w,
    gate_scale,
    up_scale,
    gate_taps,
    up_taps,
    gate_bias,
    up_bias,
    down_w,
    down_scale,
):
    resid = tokens[0].astype(jnp.float32)
    normed_in = norm_rows(resid, mix_gain).astype(jnp.bfloat16)
    all_rows = lax.all_gather(normed_in, "tp", axis=0, tiled=True)
    whole_outgate, whole_ingate, whole_value, whole_gate, whole_up, whole_proj, whole_down = (
        gather_packed(
            (
                out_gate_scale,
                in_gate_scale,
                value_scale,
                gate_scale,
                up_scale,
                proj_scale,
                down_scale,
            ),
            "fs",
            (0, 0, 0, 0, 0, 0, 0),
        )
    )
    outgate_rows, ingate_rows, value_rows = side_by_side(
        (
            out_gate_w.astype(jnp.bfloat16),
            in_gate_w.astype(jnp.bfloat16),
            value_w.astype(jnp.bfloat16),
        ),
        "fs",
        0,
        1,
    )
    out_gate = (
        jnp.dot(all_rows, outgate_rows, preferred_element_type=jnp.float32) * whole_outgate
    ).astype(jnp.bfloat16)
    in_gate = (
        jnp.dot(all_rows, ingate_rows, preferred_element_type=jnp.float32) * whole_ingate
    ).astype(jnp.bfloat16)
    value_in = (
        jnp.dot(all_rows, value_rows, preferred_element_type=jnp.float32) * whole_value
    ).astype(jnp.bfloat16)
    mixed_in = in_gate.astype(jnp.float32) * value_in.astype(jnp.float32)
    conv_out = (out_gate.astype(jnp.float32) * causal_taps(mixed_in, mix_taps)).astype(jnp.bfloat16)
    conv_float = conv_out.astype(jnp.float32)
    channels = conv_float.shape[1] * lax.axis_size("tp")
    sumsq = of_everyone(jnp.sum(conv_float * conv_float, axis=1), "tp")
    mixed = (conv_float * lax.rsqrt(sumsq / channels + epsilon)[:, None] * conv_gain).astype(
        jnp.bfloat16
    )
    partial_mix = (lambda piece, start: column_block(mixed, whole_proj, piece))(
        collect(out_proj_w.astype(jnp.bfloat16), "fs", 1), jnp.int32(0)
    )
    summed = summed_on_arrival(partial_mix.astype(jnp.bfloat16), "tp", 0)
    first = (resid + summed).astype(jnp.bfloat16)
    resid_two = first.astype(jnp.float32)
    normed_ffn = norm_rows(resid_two, ffn_gain).astype(jnp.bfloat16)
    ffn_all = lax.all_gather(normed_ffn, "tp", axis=0, tiled=True)
    gate_cast = gate_w.astype(jnp.bfloat16)
    up_cast = up_w.astype(jnp.bfloat16)
    pieces = side_by_side((gate_cast, up_cast), "fs", 0, 1)
    gate_sum = jnp.dot(ffn_all, pieces[0], preferred_element_type=jnp.float32)
    up_sum = jnp.dot(ffn_all, pieces[1], preferred_element_type=jnp.float32)
    gate_pre = (gate_sum * whole_gate).astype(jnp.bfloat16)
    up_pre = (up_sum * whole_up).astype(jnp.bfloat16)
    gate_act = causal_taps(gate_pre.astype(jnp.float32), gate_taps) + gate_bias
    up_act = causal_taps(up_pre.astype(jnp.float32), up_taps) + up_bias
    hidden = (jax.nn.silu(gate_act) * up_act).astype(jnp.bfloat16)
    partial_down = column_block(
        hidden, whole_down, lax.all_gather(down_w.astype(jnp.bfloat16), "fs", axis=1, tiled=True)
    )
    summed_two = summed_on_arrival(partial_down.astype(jnp.bfloat16), "tp", 0)
    return (resid_two + summed_two).astype(jnp.bfloat16)[None]


def solution(mesh):
    placed = (
        P(("rep", "fs"), "tp", None),
        P(),
        P("fs", "tp"),
        P("fs", "tp"),
        P("fs", "tp"),
        P(("tp", "fs")),
        P(("tp", "fs")),
        P(("tp", "fs")),
        P(None, "tp"),
        P("tp"),
        P("tp", "fs"),
        P("fs"),
        P(),
        P("fs", "tp"),
        P("fs", "tp"),
        P(("tp", "fs")),
        P(("tp", "fs")),
        P(None, "tp"),
        P(None, "tp"),
        P("tp"),
        P("tp"),
        P("tp", "fs"),
        P("fs"),
    )
    return jax.shard_map(
        local, mesh=mesh, in_specs=placed, out_specs=P(("rep", "fs"), "tp", None), check_vma=False
    )
```

profile of v0, /device:TPU:1, one launch (start us, length us, event | category | flops | bytes accessed | tf_op | source)
XLA Modules:
  0.0 658.0 jit_solution(3495908413047542810)
XLA Ops:
  6.5 2.1 fusion.11
  8.7 0.0 copy-start.15
  8.7 0.0 copy-start.16
  8.7 0.0 copy-start.19
  8.7 0.0 copy-start.20
  8.8 0.0 copy-start.13
  8.8 3.5 fusion.13
  12.3 0.0 all-gather.7.cloned.1.call-update
  12.4 0.0 all-gather.9.cloned.1.call-start
  12.5 0.7 pad_maximum_fusion.1
  13.2 0.0 all-gather.9.cloned.1.call-update
  13.2 0.7 dynamic-slice
  14.6 0.1 concatenate.10
  14.7 0.3 dynamic-update-slice
  15.0 135.7 %all-reduce.3 = f32[8448]{0:T(1024)S(1)} all-reduce(f32[8448]{0:T(1024)S(1)} %dynamic-update-slice), channel_id=2, replica_groups=mesh['rep'=2,'fs'=32,'tp'=2] {'fs'}, use_global_device_ids=true, to_apply=%add.3 | all-reduce | flops 8448 | bytes 67584
  150.7 0.1 reshape.57
  150.8 0.1 fusion.57
  150.9 0.1 mul.243
  150.9 0.1 mul.240
  151.0 0.1 mul.235
  151.2 0.0 all-gather.7.cloned.1.call-done
  151.2 25.6 %all-gather.9.cloned.1.call-done = bf16[2048,1536]{1,0:T(8,128)(2,1)} async-done(((bf16[64,1536]{1,0:T(8,128)(2,1)}), bf16[2048,1536]{1,0:T(8,128)(2,1)}) %all-gather.9.cloned.1.call-update) | async-done | bytes 6291472 | tf_op jit(solution)/shard_map/all_gather | solution.py:28
  176.8 5.4 multiply_convert_fusion.6
  182.1 0.5 copy-done.23
  182.6 2.4 convert_multiply_fusion.4
  185.0 3.1 fusion.32
  188.1 0.0 copy-start.27
  188.1 24.5 %all_to_all.21 = f32[2,1,1024]{2,1,0:T(1,128)S(1)} all-to-all(f32[2,1,1024]{2,1,0:T(1,128)S(1)} %broadcast_in_dim.4), channel_id=1, replica_groups=mesh['rep'=2,'fs'=32,'tp'=2] {'tp'}, dimensions={0} | all-to-all | bytes 16384 | tf_op jit(solution)/shard_map/all_to_all | solution.py:34
  212.7 1.6 broadcast_in_dim.5
  214.2 6.8 %all-to-all-start.1 = ((bf16[32,512,64]{1,2,0:T(8,128)(2,1)}), bf16[32,512,64]{1,2,0:T(8,128)(2,1)S(1)}, u32[]{:S(2)}, u32[]{:S(2)}) async-start(bf16[32,512,64]{1,2,0:T(8,128)(2,1)} %broadcast_in_dim.5), calls=%async_computation.1 | async-start | bytes 4194304 | tf_op jit(solution)/shard_map/all_to_all | solution.py:34
  221.0 0.0 all-gather.11.cloned.1.call-start
  221.0 0.1 fusion.58
  221.1 0.1 mul.260
  221.2 26.7 %all-to-all-done.1 = bf16[32,512,64]{1,2,0:T(8,128)(2,1)S(1)} async-done(((bf16[32,512,64]{1,2,0:T(8,128)(2,1)}), bf16[32,512,64]{1,2,0:T(8,128)(2,1)S(1)}, u32[]{:S(2)}, u32[]{:S(2)}) %all-to-all-start.1) | async-done | bytes 2097184 | tf_op jit(solution)/shard_map/all_to_all | solution.py:34
  247.9 2.6 multiply_convert_fusion.1
  250.5 8.9 %all_to_all.22 = bf16[2,512,2048]{2,1,0:T(8,128)(2,1)S(1)} all-to-all(bf16[2,512,2048]{2,1,0:T(8,128)(2,1)S(1)} %bitcast.45), channel_id=1, replica_groups=mesh['rep'=2,'fs'=32,'tp'=2] {'tp'}, dimensions={0} | all-to-all | bytes 8388608 | tf_op jit(solution)/shard_map/all_to_all | solution.py:54
  259.4 1.0 convert_reduce_fusion.1
  260.4 0.6 copy-done.2
  261.0 0.7 fusion.16
  261.7 1.3 copy-done
  263.0 2.0 fusion.18
  265.1 0.0 all-gather.11.cloned.1.call-update
  265.1 0.0 all-gather.13.cloned.1.call-start
  265.2 0.8 pad_maximum_fusion
  266.0 0.0 all-gather.13.cloned.1.call-update
  266.0 0.0 all-gather.15.cloned.1.call-start
  266.1 0.7 convert_element_type.142
  266.8 0.0 all-gather.15.cloned.1.call-update
  266.8 0.1 fusion.56
  266.9 0.1 mul.270
  267.0 0.1 mul.283
  267.1 0.1 mul.294
  267.2 0.1 slice_reduce_fusion.2
  267.2 13.0 %all-gather.11.cloned.1.call-done = bf16[1024,2048]{1,0:T(8,128)(2,1)} async-done(((bf16[512,2048]{1,0:T(8,128)(2,1)}), bf16[1024,2048]{1,0:T(8,128)(2,1)}) %all-gather.11.cloned.1.call-update) | async-done | bytes 4194320 | tf_op jit(solution)/shard_map/all_gather | solution.py:153
  280.3 155.1 %all-gather.13.cloned.1.call-done = bf16[2048,2816]{1,0:T(8,128)(2,1)} async-done(((bf16[64,2816]{1,0:T(8,128)(2,1)}), bf16[2048,2816]{1,0:T(8,128)(2,1)}) %all-gather.13.cloned.1.call-update) | async-done | bytes 11534352 | tf_op jit(solution)/shard_map/all_gather | solution.py:28
  435.4 11.8 %fusion.20 = f32[1024,1408]{1,0:T(8,128)} fusion(bf16[1024,2048]{1,0:T(8,128)(2,1)} %all-gather.11.cloned.1.call-done, bf16[2048,2816]{1,0:T(8,128)(2,1)} %all-gather.13.cloned.1.call-done, f32[1408]{0:T(1024)S(1)} %mul.270), kind=kOutput, calls=%fused_computation.28 | convolution fusion | flops 5909905408 | bytes 15734272 | tf_op jit(solution)/shard_map/dot_general | solution.py:157
  447.2 0.0 copy-start.26
  447.2 8.5 %fusion.23 = f32[1024,1408]{1,0:T(8,128)} fusion(bf16[1024,2048]{1,0:T(8,128)(2,1)S(1)} %copy-done.24, bf16[2048,2816]{1,0:T(8,128)(2,1)S(1)} %copy-done.21, f32[1408]{0:T(1024)S(1)} %mul.283), kind=kOutput, calls=%fused_computation.29 | convolution fusion | flops 5909905408 | bytes 15736832 | tf_op jit(solution)/shard_map/dot_general | solution.py:158
  455.7 139.5 %all-gather.15.cloned.1.call-done = bf16[1408,2048]{0,1:T(8,128)(2,1)} async-done(((bf16[1408,64]{0,1:T(8,128)(2,1)}), bf16[1408,2048]{0,1:T(8,128)(2,1)}) %all-gather.15.cloned.1.call-update) | async-done | bytes 5767184 | tf_op jit(solution)/shard_map/all_gather | solution.py:165
  595.2 23.3 %multiply_convert_fusion = bf16[1024,2048]{1,0:T(8,128)(2,1)} fusion(bf16[1408,2048]{0,1:T(8,128)(2,1)} %all-gather.15.cloned.1.call-done, f32[2048]{0:T(1024)S(1)} %mul.294, f32[1024,1408]{1,0:T(8,128)} %fusion.23, f32[1024,1408]{1,0:T(8,128)} %fusion.20, f32[1408]{0:T(1024)S(1)} %copy-done.25, f32[1408]{0:T(1024)S(1)} %get-tuple-element.9, ...), kind=kOutput, calls=%fused_computation.1 | convolution fusion | flops 5935726592 | bytes 21549056 | tf_op jit(solution)/shard_map/dot_general | solution.py:73
  618.5 28.2 %all_to_all.23 = bf16[2,512,2048]{2,1,0:T(8,128)(2,1)S(1)} all-to-all(bf16[2,512,2048]{2,1,0:T(8,128)(2,1)} %bitcast.44), channel_id=1, replica_groups=mesh['rep'=2,'fs'=32,'tp'=2] {'tp'}, dimensions={0} | all-to-all | bytes 8388608 | tf_op jit(solution)/shard_map/all_to_all | solution.py:54
  646.7 1.0 convert_reduce_fusion
  647.7 1.2 copy-done.1
  648.9 2.5 fusion.19
  (61 shorter events, 0.3 us)
Async XLA Ops:
  6.5 5.9 copy-start.6
  6.5 5.9 copy-start.7
  6.5 5.9 copy-start.8
  6.5 144.6 %all-gather.7.cloned.1.call-start = ((), (), s32[]{:S(2)}) async-start(), calls=%async_computation.4 | async-start | bytes 6291456 | tf_op jit(solution)/shard_map/all_gather | solution.py:103
  8.7 4.5 copy-start.28
  8.7 5.9 copy-start.14
  8.7 5.9 copy-start.15
  8.7 5.9 copy-start.16
  8.7 5.9 copy-start.17
  8.7 5.9 copy-start.18
  8.7 5.9 copy-start.19
  8.7 5.9 copy-start.20
  8.8 142.3 %copy-start.9 = (f32[512,64]{0,1:T(8,128)S(1)}, f32[512,64]{0,1:T(8,128)}, u32[]{:S(2)}) copy-start(f32[512,64]{0,1:T(8,128)} %param.33) | copy-start | bytes 393220
  8.8 142.4 %copy-start.13 = (f32[3,512]{1,0:T(4,128)S(1)}, f32[3,512]{1,0:T(4,128)}, u32[]{:S(2)}) copy-start(f32[3,512]{1,0:T(4,128)} %param.31) | copy-start | bytes 18436
  12.4 164.4 %all-gather.9.cloned.1.call-start = ((), (), s32[]{:S(2)}) async-start(), calls=%async_computation.5 | async-start | bytes 6488064 | tf_op jit(solution)/shard_map/all_gather | solution.py:28
  176.8 5.4 copy-start.22
  176.8 5.9 copy-start.23
  188.1 59.8 %copy-start.27 = (f32[512]{0:T(512)S(1)}, f32[512]{0:T(512)}, u32[]{:S(2)}) copy-start(f32[512]{0:T(512)} %param.32) | copy-start | bytes 6148
  214.2 33.7 %all-to-all-start.1 = ((bf16[32,512,64]{1,2,0:T(8,128)(2,1)}), bf16[32,512,64]{1,2,0:T(8,128)(2,1)S(1)}, u32[]{:S(2)}, u32[]{:S(2)}) async-start(bf16[32,512,64]{1,2,0:T(8,128)(2,1)} %broadcast_in_dim.5), calls=%async_computation.1 | async-start | bytes 4194304 | tf_op jit(solution)/shard_map/all_to_all | solution.py:34
  221.0 59.3 %all-gather.11.cloned.1.call-start = ((), (), s32[]{:S(2)}) async-start(), calls=%async_computation.6 | async-start | bytes 6291456 | tf_op jit(solution)/shard_map/all_gather | solution.py:153
  259.4 1.6 copy-start.2
  261.0 2.0 copy-start
  261.0 2.0 copy-start.12
  263.0 2.1 copy-start.3
  263.0 2.2 copy-start.4
  265.1 1.0 copy-start.5
  265.1 2.1 copy-start.10
  265.1 2.1 copy-start.11
  265.1 170.3 %all-gather.13.cloned.1.call-start = ((), (), s32[]{:S(2)}) async-start(), calls=%async_computation.7 | async-start | bytes 11894784 | tf_op jit(solution)/shard_map/all_gather | solution.py:28
  266.0 329.2 %all-gather.15.cloned.1.call-start = ((), (), s32[]{:S(2)}) async-start(), calls=%async_computation.8 | async-start | bytes 5947392 | tf_op jit(solution)/shard_map/all_gather | solution.py:165
  435.4 11.8 %copy-start.21 = (bf16[2048,2816]{1,0:T(8,128)(2,1)S(1)}, bf16[2048,2816]{1,0:T(8,128)(2,1)}, u32[]{:S(2)}) copy-start(bf16[2048,2816]{1,0:T(8,128)(2,1)} %all-gather.13.cloned.1.call-done) | copy-start | bytes 34603012
  435.4 11.8 %copy-start.24 = (bf16[1024,2048]{1,0:T(8,128)(2,1)S(1)}, bf16[1024,2048]{1,0:T(8,128)(2,1)}, u32[]{:S(2)}) copy-start(bf16[1024,2048]{1,0:T(8,128)(2,1)} %all-gather.11.cloned.1.call-done) | copy-start | bytes 12582916
  447.2 148.0 %copy-start.25 = (f32[1408]{0:T(1024)S(1)}, f32[1408]{0:T(1024)}, u32[]{:S(2)}) copy-start(f32[1408]{0:T(1024)} %param.43) | copy-start | bytes 16900
  447.2 148.0 %copy-start.26 = (f32[1408]{0:T(1024)S(1)}, f32[1408]{0:T(1024)}, u32[]{:S(2)}) copy-start(f32[1408]{0:T(1024)} %param.42) | copy-start | bytes 16900
  646.7 2.2 copy-start.1
Sparse Core Ops, SparseCore 0:
  12.5 19.9 all-gather.6
  34.1 142.5 all-gather.8
  265.2 15.0 all-gather.10
  281.8 153.5 all-gather.12
  436.9 158.2 all-gather.14
where the time goes:
time: 658 us
  waiting for transfers between devices  360 us (55%)
  blocking collectives  197 us (30%)
  matrix products  57 us (9%)
  other arithmetic  15.1 us (2%)
  between operations  14.3 us (2%)
  local copies, waits for them, and re-layouts  7.36 us (1%)
  starting transfers between devices  6.92 us (1%)
    all_gather x2, waiting for transfers between devices, side_by_side(): filled = lax.all_gather(both, axis, axis=dim, tiled=True)  181 us
    all_gather x1, waiting for transfers between devices, local(): lax.all_gather(down_w.astype(jnp.bfloat16), 'fs', axis=1, tiled=True)  139 us
    unnamed x1, blocking collectives  136 us
    all_to_all x2, blocking collectives, summed_on_arrival(): parts = lax.all_to_all(split_up(shard, dim, size), axis, 0, 0, tiled=True)  37.1 us
    all_to_all x1, waiting for transfers between devices, from_everyone(): lax.all_to_all(jnp.broadcast_to(shard[None], (size, *shard.shape)), axis,...  26.7 us
    dot_general x2, matrix products, column_block(): return jnp.dot(left, piece, preferred_element_type=jnp.float32) * scale_all  25.9 us
    all_to_all x1, blocking collectives, from_everyone(): lax.all_to_all(jnp.broadcast_to(shard[None], (size, *shard.shape)), axis,...  24.5 us
  transfers between devices with their start and end apart: 6, of which 5 were waited for; matrix products, arithmetic and copies ran while one was open for 4% of the time, Pallas kernels for 0%

commit v1 on v0

v1 whole, which is shorter than its diff:
```python
import jax
import jax.numpy as jnp
from jax import lax
from jax.experimental import pallas as pl
from jax.experimental.pallas import tpu as pltpu
from jax.sharding import PartitionSpec as P

EPS = 1e-06
MESH = pl.DeviceIdType.MESH
BF, F32 = jnp.bfloat16, jnp.float32
RATE = 46.65e3
TM = 256

PARTS = (
    ("s", 0, "xyz"),
    ("m", 3, "xyz"),
    ("m", 3, "zxy"),
    ("m", 3, "yxz"),
    ("m", 3, "zyx"),
    ("o", 4, "xyz"),
    ("g", 6, "yxz"),
    ("g", 6, "zxy"),
    ("g", 6, "zyx"),
    ("g", 4, "xyz"),
    ("d", 4, "zxy"),
    ("d", 4, "yxz"),
    ("d", 3, "zyx"),
)


class Copy:
    def __init__(self, part, stage, axis, sign, spec, rows, deps, nbytes):
        self.part, self.stage, self.axis, self.sign = part, stage, axis, sign
        self.spec, self.rows, self.deps, self.nbytes = spec, rows, deps, nbytes
        self.key = (part, stage, 0 if sign > 0 else 1)


def copies_of(part, kind, blocks, order):
    have = dict(x="own", y="own", z="own")
    size = dict(x=4, y=4, z=2)
    row = 512 if kind == "s" else blocks * 256
    whole, halves = ((0, 8), ((0, 8), None)) if kind == "s" else ((0, 64), ((0, 32), (32, 32)))
    made, stage, before = [], 0, []

    def add(stage, axis, sign, spec, rows, deps):
        count = 1
        for a in "xyz":
            count *= size[a] if spec[a] == "all" else 1
        made.append(Copy(part, stage, axis, sign, dict(spec), rows, list(deps), count * rows[1] * row))
        return made[-1].key

    for axis in order:
        done = []
        if axis == "z":
            for sign, rows in zip((1, -1), halves):
                if rows:
                    done.append(add(stage, axis, sign, have, rows, before))
            stage += 1
        else:
            firsts = [add(stage, axis, sign, have, whole, before) for sign in (1, -1)]
            done += firsts
            for sign, first, rows in zip((1, -1), firsts, halves):
                if rows:
                    done.append(add(stage + 1, axis, sign, {**have, axis: -sign}, rows, before + [first]))
            stage += 2
        before = before + done
        have[axis] = "all"
    return made, before


def plan(segments, backlog=4.0, latency=2.4, issue=0.06, start=2.0):
    todo, ends = [], []
    for p, (kind, blocks, order) in enumerate(PARTS):
        made, end = copies_of(p, kind, blocks, order)
        todo += made
        ends.append(end)
    arrive, link = {}, {(a, s): 0.0 for a in "xyz" for s in (1, -1)}
    out, now, seg = [], start, 0
    while todo or seg < len(segments):
        moved = True
        while moved:
            moved = False
            for op in todo:
                if all(arrive.get(d, 1e9) <= now for d in op.deps) and link[op.axis, op.sign] - now < backlog:
                    link[op.axis, op.sign] = max(now, link[op.axis, op.sign]) + op.nbytes / RATE
                    arrive[op.key] = link[op.axis, op.sign] + latency
                    out.append(("send", op, now))
                    now += issue
                    todo.remove(op)
                    moved = True
                    break
        if seg < len(segments):
            name, us, needs = segments[seg]
            if all(arrive.get(k, 1e9) <= now for p in needs for k in ends[p]):
                out.append(("run", segments[seg], now))
                now += us
                seg += 1
                continue
        later = [v for v in arrive.values() if v > now]
        later += [v - backlog + 1e-6 for v in link.values() if v - backlog + 1e-6 > now]
        if not later:
            break
        now = min(later)
    return out, ends


def parts_of(kind):
    return [p for p, part in enumerate(PARTS) if part[0] == kind]


def segments_of():
    out = [("norm", 4.0, [])]
    for c, p in enumerate(parts_of("m")):
        out.append((("m", c, p), 2.4, [p] + parts_of("s")))
    out += [(("o", h), 1.5, parts_of("o")) for h in range(2)]
    out += [(("f", i), 1.5, []) for i in range(4)]
    j = 0
    for p in parts_of("g"):
        for b in range(PARTS[p][1] // 2):
            out.append((("g", j, p, b), 2.0, [p]))
            j += 1
    d = parts_of("d")
    k = 0
    for n, p in enumerate(d[:-1]):
        out += [(("d", p, k, n == 0, h), 1.4, [p]) for h in range(2)]
        k += PARTS[p][1] * 128
    out += [(("e", d[-1], k), 4.0, d[-1:])]
    return out


def dot_nt(a, b):
    return lax.dot_general(a, b, (((1,), (1,)), ((), ())), preferred_element_type=F32)


def shifted_sum(prev, cur, taps):
    both = jnp.concatenate([prev, cur], axis=0)
    one = pltpu.roll(both, 1, 0)[8:]
    two = pltpu.roll(both, 2, 0)[8:]
    return taps[2:3] * cur + taps[1:2] * one + taps[0:1] * two


def kernel(*refs):
    n = len(PARTS)
    (tok, own, sown, mixg, mtaps, cgain, fgain, gtaps, utaps, gbias, ubias, out) = refs[:12]
    bufs = refs[12 : 12 + n]
    (tt, xx, cc, ss, ssr, ps, pr, hh, yy, dr, sc, ssem, rsem, lsem, tsem, trsem) = refs[12 + n :]
    rep, fs, tp = lax.axis_index("rep"), lax.axis_index("fs"), lax.axis_index("tp")
    z, y, x = fs // 16, lax.rem(fs // 4, 4), lax.rem(fs, 4)
    pos = dict(x=x, y=y, z=z)
    mate = (rep, fs, 1 - tp)

    def beside(axis, sign):
        if axis == "x":
            return (rep, z * 16 + y * 4 + lax.rem(x + sign + 4, 4), tp)
        if axis == "y":
            return (rep, z * 16 + lax.rem(y + sign + 4, 4) * 4 + x, tp)
        far = lax.rem(rep * 2 + z + sign + 4, 4)
        return (far // 2, lax.rem(far, 2) * 16 + y * 4 + x, tp)

    local, at = [], 0
    for p, (kind, blocks, _) in enumerate(PARTS):
        src = sown if kind == "s" else own.at[:, pl.ds(at, blocks * 128)]
        local.append(pltpu.make_async_copy(src, bufs[p].at[z, y, x], lsem.at[p]))
        at += blocks * 128
    mine = pl.multiple_of(tp * 512, 512)
    other = pl.multiple_of((1 - tp) * 512, 512)
    local.append(pltpu.make_async_copy(tok.at[0], tt.at[pl.ds(mine, 512)], lsem.at[n]))
    for c in local:
        c.start()

    barrier = pltpu.get_barrier_semaphore()
    for axis in "xyz":
        for sign in (1, -1):
            pl.semaphore_signal(barrier, inc=1, device_id=beside(axis, sign), device_id_type=MESH)
    pl.semaphore_signal(barrier, inc=1, device_id=mate, device_id_type=MESH)
    pl.semaphore_wait(barrier, 7)

    def to_mate(src, dst, k):
        return pltpu.make_async_remote_copy(
            src_ref=src, dst_ref=dst, send_sem=tsem.at[k], recv_sem=trsem.at[k], device_id=mate, device_id_type=MESH
        )

    tokens_over = to_mate(tok.at[0], tt.at[pl.ds(mine, 512)], 0)
    tokens_over.start()
    for c in local:
        c.wait()

    def where(spec, axis):
        v = spec[axis]
        if v == "all":
            return pl.ds(0, 2 if axis == "z" else 4)
        if v == "own":
            return pl.ds(pos[axis], 1)
        return pl.ds(lax.rem(pos[axis] + v + 4, 4), 1)

    def rows_of(i, size=TM):
        return pl.ds(pl.multiple_of(i * size, size), size)

    def whole(p, cols):
        return bufs[p][:, :, :, :, cols].reshape(2048, -1)

    def run_norm():
        tokens_over.wait()

        @pl.loop(0, 1024 // 64)
        def _(i):
            r = rows_of(i, 64)
            v = tt[r, :].astype(F32)
            v = v * lax.rsqrt(jnp.mean(v * v, axis=1, keepdims=True) + EPS) * mixg[...]
            xx[r, :] = v.astype(BF)

    def run_scales(p):
        lane = lax.broadcasted_iota(jnp.int32, (1, 128), 1)
        for k in range(3):
            for b in range(4):
                total = None
                for d in range(8 * b, 8 * b + 8):
                    v = bufs[p][d // 16, d // 4 % 4, d % 4, k : k + 1, :]
                    total = v if total is None else total + v
                sc[k : k + 1, b * 128 : b * 128 + 128] = total
        for k in range(3, 5):
            for b in range(11):
                total = jnp.zeros((1, 128), F32)
                for d in range(32):
                    low, high = max(44 * d - 128 * b, 0), min(44 * d + 44 - 128 * b, 128)
                    if low < high:
                        v = bufs[p][d // 16, d // 4 % 4, d % 4, k : k + 1, :]
                        total = jnp.where((lane >= low) & (lane < high), v, total)
                sc[k : k + 1, b * 128 : b * 128 + 128] = total

    def run_m(c, p):
        cols = slice(c * 128, c * 128 + 128)
        taps, gain = mtaps[:, cols], cgain[:, cols]
        s_out, s_in, s_val = (sc[k : k + 1, cols] for k in range(3))
        s_both = s_in * s_val

        def tile(i, prev):
            r = rows_of(i)
            acc = jnp.dot(xx[r, :], whole(p, slice(None)), preferred_element_type=F32)
            cur = acc[:, 128:256] * acc[:, 256:384] * s_both
            conv = acc[:, 0:128] * s_out * shifted_sum(prev, cur, taps)
            if c == 0:
                ss[r, :] = conv * conv
            else:
                ss[r, :] += conv * conv
            cc[r, cols] = (conv * gain).astype(BF)
            return cur[TM - 8 :]

        lax.fori_loop(0, 1024 // TM, tile, jnp.zeros((8, 128), F32))

    def p_over(i):
        return to_mate(ps.at[rows_of(i)], pr.at[rows_of(i)], 2 + i)

    squares_over = to_mate(ss, ssr, 1)

    def run_o(h):
        (p,) = parts_of("o")

        @pl.loop(2 * h, 2 * h + 2)
        def _(i):
            r = rows_of(i)

            @pl.loop(0, 4)
            def _(q):
                w = bufs[p][q // 2, pl.ds(lax.rem(q, 2) * 2, 2)].reshape(512, 512)
                ps[r, pl.ds(pl.multiple_of(q * 512, 512), 512)] = dot_nt(cc[r, :], w).astype(BF)

        if h == 0:
            squares_over.start()
        else:
            for i in range(4):
                p_over(i).start()

    def run_f(i):
        if i == 0:
            squares_over.wait()
        p_over(i).wait()

        @pl.loop(i * (TM // 64), (i + 1) * (TM // 64))
        def _(k):
            r = rows_of(k, 64)
            row = lax.rsqrt(jnp.sum(ss[r, :] + ssr[r, :], axis=1, keepdims=True) * (1.0 / 1024) + EPS)
            v = tt[r, :].astype(F32) + row * (ps[r, :].astype(F32) + pr[r, :].astype(F32))
            b = v.astype(BF)
            tt[r, :] = b
            v = b.astype(F32)
            v = v * lax.rsqrt(jnp.mean(v * v, axis=1, keepdims=True) + EPS) * fgain[...]
            xx[r, :] = v.astype(BF)

    def run_g(j, p, b):
        cols = slice(j * 128, j * 128 + 128)
        tg, tu, bg, bu = gtaps[:, cols], utaps[:, cols], gbias[:, cols], ubias[:, cols]
        sg, su = sc[3:4, cols], sc[4:5, cols]

        def tile(i, prev):
            r = rows_of(i)
            acc = jnp.dot(xx[r, :], whole(p, slice(b * 256, b * 256 + 256)), preferred_element_type=F32)
            g, u = acc[:, :128] * sg, acc[:, 128:] * su
            ga = shifted_sum(prev[0], g, tg) + bg
            ua = shifted_sum(prev[1], u, tu) + bu
            hh[r, cols] = (ga / (1.0 + jnp.exp(-ga)) * ua).astype(BF)
            return g[TM - 8 :], u[TM - 8 :]

        zero = jnp.zeros((8, 128), F32)
        lax.fori_loop(0, 1024 // TM, tile, (zero, zero))

    def d_tile(r, p, k, q):
        w = bufs[p][q // 2, pl.ds(lax.rem(q, 2) * 2, 2)].reshape(512, -1)
        return dot_nt(hh[r, pl.ds(k, w.shape[1])], w)

    def run_d(p, k, first, h):
        @pl.loop(2 * h, 2 * h + 2)
        def _(i):
            r = rows_of(i)

            @pl.loop(0, 4)
            def _(q):
                c = pl.ds(pl.multiple_of(q * 512, 512), 512)
                if first:
                    yy[r, c] = d_tile(r, p, k, q)
                else:
                    yy[r, c] += d_tile(r, p, k, q)

    def d_over(i):
        return to_mate(ps.at[rows_of(i)], dr.at[rows_of(i)], 6 + i)

    def run_e(p, k):
        for i in range(2):
            r = pl.ds(pl.multiple_of(other + i * TM, TM), TM)

            @pl.loop(0, 4)
            def _(q):
                c = pl.ds(pl.multiple_of(q * 512, 512), 512)
                ps[pl.ds(i * TM, TM), c] = (yy[r, c] + d_tile(r, p, k, q)).astype(BF)

            d_over(i).start()
        for i in range(2):
            r = pl.ds(pl.multiple_of(mine + i * TM, TM), TM)

            @pl.loop(0, 4)
            def _(q):
                c = pl.ds(pl.multiple_of(q * 512, 512), 512)
                yy[r, c] += d_tile(r, p, k, q)

        written = []
        for i in range(2):
            d_over(i).wait()

            @pl.loop(0, TM // 64)
            def _(q):
                r = pl.ds(pl.multiple_of(mine + i * TM + q * 64, 64), 64)
                o = pl.ds(pl.multiple_of(i * TM + q * 64, 64), 64)
                xx[o, :] = (tt[r, :].astype(F32) + yy[r, :] + dr[o, :].astype(F32)).astype(BF)

            w = pltpu.make_async_copy(xx.at[pl.ds(i * TM, TM)], out.at[0, pl.ds(i * TM, TM)], lsem.at[i])
            w.start()
            written.append(w)
        for w in written:
            w.wait()

    steps, ends = plan(segments_of())
    started, got = {}, set()

    def arrived(keys):
        for key in keys:
            if key not in got:
                got.add(key)
                started[key].wait_recv()

    scaled = False
    for what, it, _ in steps:
        if what == "send":
            arrived(it.deps)
            ref = bufs[it.part].at[where(it.spec, "z"), where(it.spec, "y"), where(it.spec, "x"), pl.ds(*it.rows)]
            c = pltpu.make_async_remote_copy(
                src_ref=ref,
                dst_ref=ref,
                send_sem=ssem.at[it.key],
                recv_sem=rsem.at[it.key],
                device_id=beside(it.axis, it.sign),
                device_id_type=MESH,
            )
            c.start()
            started[it.key] = c
            continue
        name, _, needs = it
        for p in needs:
            arrived(ends[p])
        if name == "norm":
            run_norm()
            continue
        if name[0] == "m" and not scaled:
            scaled = True
            run_scales(parts_of("s")[0])
        dict(m=run_m, o=run_o, f=run_f, g=run_g, d=run_d, e=run_e)[name[0]](*name[1:])
    for c in started.values():
        c.wait_send()


def placed_row(values, width):
    at = lax.rem(lax.axis_index("fs") * width, 128)
    row = lax.dynamic_update_slice(jnp.zeros((256,), F32), values, (at,))
    return row[:128] + row[128:]


def local(
    tokens, mix_gain, out_gate_w, in_gate_w, value_w, out_gate_scale, in_gate_scale, value_scale, mix_taps, conv_gain,
    out_proj_w, proj_scale, ffn_gain, gate_w, up_w, gate_scale, up_scale, gate_taps, up_taps, gate_bias, up_bias, down_w, down_scale,
):
    pieces = []
    for c in range(4):
        pieces += [w[:, c * 128 : c * 128 + 128] for w in (out_gate_w, in_gate_w, value_w)]
    pieces.append((out_proj_w * proj_scale).T)
    for j in range(11):
        pieces += [w[:, j * 128 : j * 128 + 128] for w in (gate_w, up_w)]
    pieces.append((down_w * down_scale).T)
    own = jnp.concatenate([p.astype(BF) for p in pieces], axis=1)
    rows = [placed_row(v, 16) for v in (out_gate_scale, in_gate_scale, value_scale)]
    rows += [placed_row(v, 44) for v in (gate_scale, up_scale)] + [jnp.zeros((128,), F32)] * 3
    sown = jnp.stack(rows)
    n = len(PARTS)
    hbm, vmem = pl.BlockSpec(memory_space=pl.ANY), pl.BlockSpec(memory_space=pltpu.VMEM)
    bufs = [
        pltpu.VMEM((2, 4, 4, 8, 128), F32) if kind == "s" else pltpu.VMEM((2, 4, 4, 64, blocks * 128), BF)
        for kind, blocks, _ in PARTS
    ]
    dma = pltpu.SemaphoreType.DMA
    return pl.pallas_call(
        kernel,
        out_shape=jax.ShapeDtypeStruct((1, 512, 2048), BF),
        in_specs=[hbm, hbm, hbm] + [vmem] * 8,
        out_specs=hbm,
        scratch_shapes=bufs
        + [
            pltpu.VMEM((1024, 2048), BF),
            pltpu.VMEM((1024, 2048), BF),
            pltpu.VMEM((1024, 512), BF),
            pltpu.VMEM((1024, 128), F32),
            pltpu.VMEM((1024, 128), F32),
            pltpu.VMEM((1024, 2048), BF),
            pltpu.VMEM((1024, 2048), BF),
            pltpu.VMEM((1024, 1408), BF),
            pltpu.VMEM((1024, 2048), F32),
            pltpu.VMEM((512, 2048), BF),
            pltpu.VMEM((8, 1408), F32),
            dma((n, 5, 2)),
            dma((n, 5, 2)),
            dma((n + 1,)),
            dma((8,)),
            dma((8,)),
        ],
        compiler_params=pltpu.CompilerParams(collective_id=0, has_side_effects=True, vmem_limit_bytes=67043328),
        name="layer",
    )(
        tokens, own, sown, mix_gain[None], mix_taps, conv_gain[None], ffn_gain[None],
        gate_taps, up_taps, gate_bias[None], up_bias[None],
    )


def solution(mesh):
    placed = (
        P(("rep", "fs"), "tp", None),
        P(),
        P("fs", "tp"),
        P("fs", "tp"),
        P("fs", "tp"),
        P(("tp", "fs")),
        P(("tp", "fs")),
        P(("tp", "fs")),
        P(None, "tp"),
        P("tp"),
        P("tp", "fs"),
        P("fs"),
        P(),
        P("fs", "tp"),
        P("fs", "tp"),
        P(("tp", "fs")),
        P(("tp", "fs")),
        P(None, "tp"),
        P(None, "tp"),
        P("tp"),
        P("tp"),
        P("tp", "fs"),
        P("fs"),
    )
    return jax.shard_map(
        local, mesh=mesh, in_specs=placed, out_specs=P(("rep", "fs"), "tp", None), check_vma=False
    )
```

time: 658 us -> 180 us (0.27)
  waiting for transfers between devices: 360 us -> 0 us
  blocking collectives: 197 us -> 0 us
  Pallas kernels: 0 us -> 142 us
  matrix products: 57 us -> 0 us
  local copies, waits for them, and re-layouts: 7.36 us -> 31.4 us
  between operations: 14.3 us -> 0.11 us
  other arithmetic: 15.1 us -> 6.25 us
  starting transfers between devices: 6.92 us -> 0 us
    all_gather x5 -> x0, waiting for transfers between devices: 333 us -> none  [the longest x2 181 us: side_by_side(): filled = lax.all_gather(both, axis, axis=dim, tiled=True)]
    pallas_call x0 -> x1, Pallas kernels: none -> 142 us  [local(): pl.pallas_call(kernel, out_shape=jax.ShapeDtypeStruct((1, 512, 2048), BF)...]
    unnamed x1 -> x0, blocking collectives: 136 us -> none
    all_to_all x3 -> x0, blocking collectives: 61.7 us -> none  [the longest x2 37.1 us: summed_on_arrival(): parts = lax.all_to_all(split_up(shard, dim, size), axis, 0, 0, tiled=True)]
    dot_general x7 -> x0, matrix products: 57 us -> none  [the longest x2 25.9 us: column_block(): return jnp.dot(left, piece, preferred_element_type=jnp.float32) * scale_all]
    all_to_all x1 -> x0, waiting for transfers between devices: 26.7 us -> none  [from_everyone(): lax.all_to_all(jnp.broadcast_to(shard[None], (size, *shard.shape)), axis,...]
    unnamed x61 -> x43, local copies, waits for them, and re-layouts: 4.71 us -> 23.8 us
    convert_element_type x10 -> x0, other arithmetic: 8.86 us -> none  [the longest x1 3.53 us: local(): normed_in = norm_rows(resid, mix_gain).astype(jnp.bfloat16)]
  transfers between devices with their start and end apart: 6 -> 0, of which waited for: 5 -> 0; matrix products, arithmetic and copies ran while one was open for 4% -> 0% of each run, Pallas kernels for 0% -> 0%
where the time goes in v1:
time: 180 us; the launch traced here: 179 us
  Pallas kernels  142 us (79%)
  local copies, waits for them, and re-layouts  31.4 us (17%)
  other arithmetic  6.25 us (3%)
    pallas_call x1, Pallas kernels, local(): pl.pallas_call(kernel, out_shape=jax.ShapeDtypeStruct((1, 512, 2048), BF)...  142 us
    unnamed x43, local copies, waits for them, and re-layouts  23.8 us
    another operation x5, other arithmetic  4.76 us
    dynamic_update_slice x5, local copies, waits for them, and re-layouts, placed_row(): row = lax.dynamic_update_slice(jnp.zeros((256,), F32), values, (at,))  4.37 us

profile of v1, /device:TPU:1, one launch (start us, length us, event | category | flops | bytes accessed | tf_op | source)
XLA Modules:
  0.0 179.5 jit_solution(10965688067050738679)
XLA Ops:
  0.0 0.0 copy-start.3
  0.0 0.0 copy-start
  0.0 0.0 copy-start.2
  0.0 0.0 copy-start.1
  0.0 1.0 dynamic_update_slice.19
  1.0 0.8 dynamic_update_slice.16
  1.9 0.8 dynamic_update_slice.17
  2.7 0.9 dynamic_update_slice.15
  3.6 0.9 dynamic_update_slice.18
  4.5 0.6 stack.27.refs_2_
  5.1 1.3 broadcast_in_dim.20.refs_9_
  6.4 1.3 broadcast_in_dim.21.refs_10_
  7.7 0.9 convert.44
  8.6 0.9 convert.45
  9.5 0.9 convert.46
  10.4 1.0 convert.47
  11.4 1.0 convert.48
  12.4 0.6 constant_dynamic-update-slice_fusion.34
  13.1 0.6 constant_dynamic-update-slice_fusion.33
  13.7 0.6 constant_dynamic-update-slice_fusion.32
  14.3 0.6 constant_dynamic-update-slice_fusion.31
  14.9 0.6 constant_dynamic-update-slice_fusion.30
  15.5 0.6 constant_dynamic-update-slice_fusion.29
  16.1 0.6 constant_dynamic-update-slice_fusion.28
  16.7 0.6 constant_dynamic-update-slice_fusion.27
  17.3 0.6 constant_dynamic-update-slice_fusion.26
  17.9 0.6 constant_dynamic-update-slice_fusion.25
  18.5 0.6 constant_dynamic-update-slice_fusion.24
  19.1 0.6 constant_dynamic-update-slice_fusion.23
  19.7 0.0 copy-done.2
  19.7 0.0 copy-done.1
  19.7 0.7 constant_dynamic-update-slice_fusion.22
  20.5 0.6 constant_dynamic-update-slice_fusion.21
  21.1 0.6 constant_dynamic-update-slice_fusion.20
  21.7 0.6 constant_dynamic-update-slice_fusion.19
  22.3 0.6 constant_dynamic-update-slice_fusion.18
  22.9 0.6 constant_dynamic-update-slice_fusion.17
  23.5 0.6 constant_dynamic-update-slice_fusion.16
  24.1 0.6 constant_dynamic-update-slice_fusion.15
  24.7 0.6 constant_dynamic-update-slice_fusion.14
  25.3 0.6 constant_dynamic-update-slice_fusion.13
  25.9 0.6 constant_dynamic-update-slice_fusion.12
  26.5 0.6 constant_dynamic-update-slice_fusion.11
  27.1 0.6 constant_dynamic-update-slice_fusion.10
  27.7 0.6 constant_dynamic-update-slice_fusion.9
  28.3 0.6 constant_dynamic-update-slice_fusion.8
  29.0 0.6 constant_dynamic-update-slice_fusion.7
  29.6 0.6 constant_dynamic-update-slice_fusion.6
  30.2 0.6 constant_dynamic-update-slice_fusion.5
  30.8 0.6 constant_dynamic-update-slice_fusion.4
  31.4 0.6 constant_dynamic-update-slice_fusion.3
  32.0 0.6 constant_dynamic-update-slice_fusion.2
  32.6 0.6 constant_dynamic-update-slice_fusion.1
  33.2 0.6 constant_dynamic-update-slice_fusion
  33.8 0.0 copy-done.3
  33.8 0.0 copy-done
  33.8 0.8 fusion.1.refs_1_
  34.6 141.8 %layer.1 = bf16[1,512,2048]{2,1,0:T(8,128)(2,1)} custom-call(bf16[1,512,2048]{2,1,0:T(8,128)(2,1)} %refs_0_.1, bf16[64,6272]{1,0:T(8,128)(2,1)} %fusion.1.refs_1_, f32[8,128]{1,0:T(8,128)} %stack.27.refs_2_, f32[1,2048]{1,0:T(1,128)} %bitcast.21, f32[3,512]{1,0:T(4,128)} %refs_4_.1, f32[1,512]{1,0:T(1,128)} %bitcast.23, f32[1,2048]{1,0:T(1,128)} %bitcast.22, ...), custom_call_target="tpu_custom_call" | custom-call | tf_op jit(solution)/shard_map/layer/pallas_call | solution.py:428
  176.3 3.2 %copy.65 = bf16[1,512,2048]{2,1,0:T(8,128)(2,1)} copy(bf16[1,512,2048]{2,1,0:T(8,128)(2,1)} %layer.1) | data formatting | bytes 4194304
  (10 shorter events, 0.0 us)
Async XLA Ops:
  0.0 33.8 %copy-start.3 = (f32[64]{0:T(128)S(1)}, f32[64]{0:T(128)}, u32[]{:S(2)}) copy-start(f32[64]{0:T(128)} %param.45) | copy-start | bytes 772
  0.0 33.8 %copy-start = (f32[1408,64]{0,1:T(8,128)S(1)}, f32[1408,64]{0,1:T(8,128)}, u32[]{:S(2)}) copy-start(f32[1408,64]{0,1:T(8,128)} %param.44) | copy-start | bytes 1081348
  0.0 19.7 %copy-start.2 = (f32[64]{0:T(128)S(1)}, f32[64]{0:T(128)}, u32[]{:S(2)}) copy-start(f32[64]{0:T(128)} %param.34) | copy-start | bytes 772
  0.0 19.7 %copy-start.1 = (f32[512,64]{0,1:T(8,128)S(1)}, f32[512,64]{0,1:T(8,128)}, u32[]{:S(2)}) copy-start(f32[512,64]{0,1:T(8,128)} %param.33) | copy-start | bytes 393220

commit v2 on v1

--- a/solution.py
+++ b/solution.py
@@ -9,22 +9,25 @@
 MESH = pl.DeviceIdType.MESH
 BF, F32 = jnp.bfloat16, jnp.float32
 RATE = 46.65e3
-TM = 256
+TM = 1024
 
 PARTS = (
     ("s", 0, "xyz"),
+    ("m", 3, "yxz"),
     ("m", 3, "xyz"),
-    ("m", 3, "zxy"),
     ("m", 3, "yxz"),
     ("m", 3, "zyx"),
     ("o", 4, "xyz"),
-    ("g", 6, "yxz"),
-    ("g", 6, "zxy"),
-    ("g", 6, "zyx"),
+    ("g", 4, "yzx"),
+    ("g", 2, "yxz"),
+    ("g", 2, "yxz"),
+    ("g", 6, "xzy"),
+    ("g", 4, "zyx"),
     ("g", 4, "xyz"),
-    ("d", 4, "zxy"),
-    ("d", 4, "yxz"),
-    ("d", 3, "zyx"),
+    ("d", 4, "xzy"),
+    ("d", 2, "yzx"),
+    ("d", 3, "xzy"),
+    ("d", 2, "yzx"),
 )
 
 
@@ -68,7 +71,7 @@
     return made, before
 
 
-def plan(segments, backlog=4.0, latency=2.4, issue=0.06, start=2.0):
+def plan(segments, backlog=5.0, latency=2.4, issue=0.06, start=2.0):
     todo, ends = [], []
     for p, (kind, blocks, order) in enumerate(PARTS):
         made, end = copies_of(p, kind, blocks, order)
@@ -108,23 +111,36 @@
     return [p for p, part in enumerate(PARTS) if part[0] == kind]
 
 
+def homes():
+    home, wide = [], []
+    for kind, blocks, _ in PARTS:
+        if kind == "m" and wide and wide[-1] == 384:
+            home.append((len(wide) - 1, 384))
+            wide[-1] = 768
+        else:
+            home.append((len(wide), 0))
+            wide.append(blocks * 128 if kind != "s" else 0)
+    return home, wide
+
+
 def segments_of():
-    out = [("norm", 4.0, [])]
-    for c, p in enumerate(parts_of("m")):
-        out.append((("m", c, p), 2.4, [p] + parts_of("s")))
-    out += [(("o", h), 1.5, parts_of("o")) for h in range(2)]
-    out += [(("f", i), 1.5, []) for i in range(4)]
+    out = [("norm", 2.4, [])]
+    m = parts_of("m")
+    for c in range(2):
+        out.append((("m", c, m[2 * c]), 3.3, m[2 * c : 2 * c + 2] + parts_of("s")))
+    out += [(("o",), 2.4, parts_of("o"))]
+    out += [(("f", i), 1.1 if i else 2.8, []) for i in range(4)]
     j = 0
     for p in parts_of("g"):
         for b in range(PARTS[p][1] // 2):
-            out.append((("g", j, p, b), 2.0, [p]))
+            out.append((("g", j, p, b), 1.45, [p]))
             j += 1
     d = parts_of("d")
     k = 0
-    for n, p in enumerate(d[:-1]):
-        out += [(("d", p, k, n == 0, h), 1.4, [p]) for h in range(2)]
+    for i, p in enumerate(d[:-1]):
+        out += [(("d", p, k, i == 0), PARTS[p][1] * 0.57, [p])]
         k += PARTS[p][1] * 128
-    out += [(("e", d[-1], k), 4.0, d[-1:])]
+    out += [(("e", d[-1], k), 5.5 + PARTS[d[-1]][1] * 0.6, d[-1:])]
     return out
 
 
@@ -141,9 +157,12 @@
 
 def kernel(*refs):
     n = len(PARTS)
-    (tok, own, sown, mixg, mtaps, cgain, fgain, gtaps, utaps, gbias, ubias, out) = refs[:12]
-    bufs = refs[12 : 12 + n]
-    (tt, xx, cc, ss, ssr, ps, pr, hh, yy, dr, sc, ssem, rsem, lsem, tsem, trsem) = refs[12 + n :]
+    (tok, wo, wi, wv, wp, wg, wu, wd, s_o, s_i, s_v, s_g, s_u, s_p, s_d) = refs[:15]
+    (mixg, mtaps, cgain, fgain, gtaps, utaps, gbias, ubias, out) = refs[15:24]
+    home, wide = homes()
+    nb = len(wide)
+    bufs = refs[24 : 24 + nb]
+    (tt, xx, cc, ss, ssr, ps, pr, hh, yy, dr, sc, wf, sf, ssem, rsem, lsem, tsem, trsem) = refs[24 + nb :]
     rep, fs, tp = lax.axis_index("rep"), lax.axis_index("fs"), lax.axis_index("tp")
     z, y, x = fs // 16, lax.rem(fs // 4, 4), lax.rem(fs, 4)
     pos = dict(x=x, y=y, z=z)
@@ -158,13 +177,12 @@
         return (far // 2, lax.rem(far, 2) * 16 + y * 4 + x, tp)
 
     local, at = [], 0
-    for p, (kind, blocks, _) in enumerate(PARTS):
-        src = sown if kind == "s" else own.at[:, pl.ds(at, blocks * 128)]
-        local.append(pltpu.make_async_copy(src, bufs[p].at[z, y, x], lsem.at[p]))
-        at += blocks * 128
+    for w in (wo, wi, wv, wp, wg, wu, wd):
+        local.append(pltpu.make_async_copy(w, wf.at[:, pl.ds(at, w.shape[1])], lsem.at[len(local)]))
+        at += w.shape[1]
     mine = pl.multiple_of(tp * 512, 512)
     other = pl.multiple_of((1 - tp) * 512, 512)
-    local.append(pltpu.make_async_copy(tok.at[0], tt.at[pl.ds(mine, 512)], lsem.at[n]))
+    local.append(pltpu.make_async_copy(tok.at[0], tt.at[pl.ds(mine, 512)], lsem.at[len(local)]))
     for c in local:
         c.start()
 
@@ -173,6 +191,37 @@
         for sign in (1, -1):
             pl.semaphore_signal(barrier, inc=1, device_id=beside(axis, sign), device_id_type=MESH)
     pl.semaphore_signal(barrier, inc=1, device_id=mate, device_id_type=MESH)
+
+    for c in local[:-1]:
+        c.wait()
+    eye = lax.broadcasted_iota(jnp.int32, (64, 64), 0) == lax.broadcasted_iota(jnp.int32, (64, 64), 1)
+    p_col, d_col = (jnp.sum(jnp.where(eye, v[...], 0.0), axis=1, keepdims=True) for v in (s_p, s_d))
+    last = {}
+    for p, (kind, blocks, _) in enumerate(PARTS):
+        first = last.get(kind, 0)
+        last[kind] = first + blocks
+        if kind == "s":
+            sf[...] = jnp.zeros((16, 128), F32)
+            for k, v in enumerate((s_o, s_i, s_v)):
+                sf[k : k + 1, 0:16] = v[...]
+            for k, v in enumerate((s_g, s_u)):
+                sf[11 + k : 12 + k, 0:44] = v[...]
+            low = pltpu.roll(sf[0:8, :], lax.rem(fs * 16, 128), 1)
+            high = pltpu.roll(sf[8:16, :], lax.rem(fs * 44, 128), 1)
+            bufs[home[p][0]][z, y, x] = low + high
+            continue
+        for b in range(blocks):
+            j = first + b
+            if kind == "m":
+                v = wf[:, pl.ds((j % 3) * 512 + j // 3 * 128, 128)]
+            elif kind == "o":
+                v = wf[:, pl.ds(1536 + j * 128, 128)] * p_col
+            elif kind == "g":
+                v = wf[:, pl.ds(2048 + (j % 2) * 1408 + j // 2 * 128, 128)]
+            else:
+                v = wf[:, pl.ds(2048 + 2816 + j * 128, 128)] * d_col
+            at = home[p][1] + b * 128
+            bufs[home[p][0]][z, y, x, :, at : at + 128] = v.astype(BF)
     pl.semaphore_wait(barrier, 7)
 
     def to_mate(src, dst, k):
@@ -182,8 +231,7 @@
 
     tokens_over = to_mate(tok.at[0], tt.at[pl.ds(mine, 512)], 0)
     tokens_over.start()
-    for c in local:
-        c.wait()
+    local[-1].wait()
 
     def where(spec, axis):
         v = spec[axis]
@@ -193,11 +241,11 @@
             return pl.ds(pos[axis], 1)
         return pl.ds(lax.rem(pos[axis] + v + 4, 4), 1)
 
-    def rows_of(i, size=TM):
+    def rows_of(i, size):
         return pl.ds(pl.multiple_of(i * size, size), size)
 
     def whole(p, cols):
-        return bufs[p][:, :, :, :, cols].reshape(2048, -1)
+        return bufs[home[p][0]][:, :, :, :, cols].reshape(2048, -1)
 
     def run_norm():
         tokens_over.wait()
@@ -215,7 +263,7 @@
             for b in range(4):
                 total = None
                 for d in range(8 * b, 8 * b + 8):
-                    v = bufs[p][d // 16, d // 4 % 4, d % 4, k : k + 1, :]
+                    v = bufs[home[p][0]][d // 16, d // 4 % 4, d % 4, k : k + 1, :]
                     total = v if total is None else total + v
                 sc[k : k + 1, b * 128 : b * 128 + 128] = total
         for k in range(3, 5):
@@ -224,59 +272,60 @@
                 for d in range(32):
                     low, high = max(44 * d - 128 * b, 0), min(44 * d + 44 - 128 * b, 128)
                     if low < high:
-                        v = bufs[p][d // 16, d // 4 % 4, d % 4, k : k + 1, :]
+                        v = bufs[home[p][0]][d // 16, d // 4 % 4, d % 4, k : k + 1, :]
                         total = jnp.where((lane >= low) & (lane < high), v, total)
                 sc[k : k + 1, b * 128 : b * 128 + 128] = total
 
     def run_m(c, p):
-        cols = slice(c * 128, c * 128 + 128)
-        taps, gain = mtaps[:, cols], cgain[:, cols]
-        s_out, s_in, s_val = (sc[k : k + 1, cols] for k in range(3))
-        s_both = s_in * s_val
+        consts = []
+        for h in range(2):
+            cols = slice(c * 256 + h * 128, c * 256 + h * 128 + 128)
+            consts.append((cols, mtaps[:, cols] * (sc[0:1, cols] * sc[1:2, cols] * sc[2:3, cols]), cgain[:, cols]))
 
         def tile(i, prev):
-            r = rows_of(i)
+            r = rows_of(i, TM)
             acc = jnp.dot(xx[r, :], whole(p, slice(None)), preferred_element_type=F32)
-            cur = acc[:, 128:256] * acc[:, 256:384] * s_both
-            conv = acc[:, 0:128] * s_out * shifted_sum(prev, cur, taps)
-            if c == 0:
-                ss[r, :] = conv * conv
-            else:
-                ss[r, :] += conv * conv
-            cc[r, cols] = (conv * gain).astype(BF)
-            return cur[TM - 8 :]
-
-        lax.fori_loop(0, 1024 // TM, tile, jnp.zeros((8, 128), F32))
-
-    def p_over(i):
-        return to_mate(ps.at[rows_of(i)], pr.at[rows_of(i)], 2 + i)
+            kept = []
+            for h, (cols, taps, gain) in enumerate(consts):
+                at = h * 384
+                cur = acc[:, at + 128 : at + 256] * acc[:, at + 256 : at + 384]
+                conv = acc[:, at : at + 128] * shifted_sum(prev[h], cur, taps)
+                if c + h == 0:
+                    ss[r, :] = conv * conv
+                else:
+                    ss[r, :] += conv * conv
+                cc[r, cols] = (conv * gain).astype(BF)
+                kept.append(cur[TM - 8 :])
+            return tuple(kept)
+
+        zero = jnp.zeros((8, 128), F32)
+        lax.fori_loop(0, 1024 // TM, tile, (zero, zero))
+
+    def p_over(q):
+        c = pl.ds(q * 512, 512)
+        return to_mate(ps.at[:, c], pr.at[:, c], 2 + q)
 
     squares_over = to_mate(ss, ssr, 1)
 
-    def run_o(h):
+    def eighths(p, q):
+        return bufs[home[p][0]][q // 2, pl.ds(q % 2 * 2, 2)].reshape(512, -1)
+
+    def run_o():
         (p,) = parts_of("o")
-
-        @pl.loop(2 * h, 2 * h + 2)
-        def _(i):
-            r = rows_of(i)
-
-            @pl.loop(0, 4)
-            def _(q):
-                w = bufs[p][q // 2, pl.ds(lax.rem(q, 2) * 2, 2)].reshape(512, 512)
-                ps[r, pl.ds(pl.multiple_of(q * 512, 512), 512)] = dot_nt(cc[r, :], w).astype(BF)
-
-        if h == 0:
-            squares_over.start()
-        else:
-            for i in range(4):
-                p_over(i).start()
+        squares_over.start()
+        for q in range(4):
+            ps[:, q * 512 : q * 512 + 512] = dot_nt(cc[...], eighths(p, q)).astype(BF)
+            if q:
+                p_over(q - 1).start()
+        p_over(3).start()
 
     def run_f(i):
         if i == 0:
             squares_over.wait()
-        p_over(i).wait()
-
-        @pl.loop(i * (TM // 64), (i + 1) * (TM // 64))
+            for q in range(4):
+                p_over(q).wait()
+
+        @pl.loop(i * 4, i * 4 + 4)
         def _(k):
             r = rows_of(k, 64)
             row = lax.rsqrt(jnp.sum(ss[r, :] + ssr[r, :], axis=1, keepdims=True) * (1.0 / 1024) + EPS)
@@ -292,10 +341,12 @@
         tg, tu, bg, bu = gtaps[:, cols], utaps[:, cols], gbias[:, cols], ubias[:, cols]
         sg, su = sc[3:4, cols], sc[4:5, cols]
 
+        tg, tu = tg * sg, tu * su
+
         def tile(i, prev):
-            r = rows_of(i)
+            r = rows_of(i, TM)
             acc = jnp.dot(xx[r, :], whole(p, slice(b * 256, b * 256 + 256)), preferred_element_type=F32)
-            g, u = acc[:, :128] * sg, acc[:, 128:] * su
+            g, u = acc[:, :128], acc[:, 128:]
             ga = shifted_sum(prev[0], g, tg) + bg
             ua = shifted_sum(prev[1], u, tu) + bu
             hh[r, cols] = (ga / (1.0 + jnp.exp(-ga)) * ua).astype(BF)
@@ -304,55 +355,40 @@
         zero = jnp.zeros((8, 128), F32)
         lax.fori_loop(0, 1024 // TM, tile, (zero, zero))
 
-    def d_tile(r, p, k, q):
-        w = bufs[p][q // 2, pl.ds(lax.rem(q, 2) * 2, 2)].reshape(512, -1)
-        return dot_nt(hh[r, pl.ds(k, w.shape[1])], w)
-
-    def run_d(p, k, first, h):
-        @pl.loop(2 * h, 2 * h + 2)
-        def _(i):
-            r = rows_of(i)
-
-            @pl.loop(0, 4)
-            def _(q):
-                c = pl.ds(pl.multiple_of(q * 512, 512), 512)
-                if first:
-                    yy[r, c] = d_tile(r, p, k, q)
-                else:
-                    yy[r, c] += d_tile(r, p, k, q)
-
-    def d_over(i):
-        return to_mate(ps.at[rows_of(i)], dr.at[rows_of(i)], 6 + i)
+    def run_d(p, k, first):
+        for q in range(4):
+            w = eighths(p, q)
+            v = dot_nt(hh[:, k : k + w.shape[1]], w)
+            c = slice(q * 512, q * 512 + 512)
+            yy[0:1024, c] = v if first else yy[0:1024, c] + v
+
+    def d_over(q):
+        c = pl.ds(q * 512, 512)
+        return to_mate(ps.at[pl.ds(0, 512), c], dr.at[:, c], 6 + q)
 
     def run_e(p, k):
-        for i in range(2):
-            r = pl.ds(pl.multiple_of(other + i * TM, TM), TM)
-
-            @pl.loop(0, 4)
-            def _(q):
-                c = pl.ds(pl.multiple_of(q * 512, 512), 512)
-                ps[pl.ds(i * TM, TM), c] = (yy[r, c] + d_tile(r, p, k, q)).astype(BF)
-
-            d_over(i).start()
-        for i in range(2):
-            r = pl.ds(pl.multiple_of(mine + i * TM, TM), TM)
-
-            @pl.loop(0, 4)
-            def _(q):
-                c = pl.ds(pl.multiple_of(q * 512, 512), 512)
-                yy[r, c] += d_tile(r, p, k, q)
-
+        own, far = pl.ds(mine, 512), pl.ds(other, 512)
+        for q in range(4):
+            w = eighths(p, q)
+            c = slice(q * 512, q * 512 + 512)
+            ps[0:512, c] = (yy[far, c] + dot_nt(hh[far, k : k + w.shape[1]], w)).astype(BF)
+            if q:
+                d_over(q - 1).start()
+        d_over(3).start()
         written = []
-        for i in range(2):
-            d_over(i).wait()
-
-            @pl.loop(0, TM // 64)
-            def _(q):
-                r = pl.ds(pl.multiple_of(mine + i * TM + q * 64, 64), 64)
-                o = pl.ds(pl.multiple_of(i * TM + q * 64, 64), 64)
-                xx[o, :] = (tt[r, :].astype(F32) + yy[r, :] + dr[o, :].astype(F32)).astype(BF)
-
-            w = pltpu.make_async_copy(xx.at[pl.ds(i * TM, TM)], out.at[0, pl.ds(i * TM, TM)], lsem.at[i])
+        for q in range(4):
+            w = eighths(p, q)
+            c = slice(q * 512, q * 512 + 512)
+            yy[own, c] += dot_nt(hh[own, k : k + w.shape[1]], w)
+            d_over(q).wait()
+
+            @pl.loop(0, 8)
+            def _(i):
+                r = pl.ds(pl.multiple_of(mine + i * 64, 64), 64)
+                o = rows_of(i, 64)
+                xx[o, c] = (tt[r, c].astype(F32) + yy[r, c] + dr[o, c].astype(F32)).astype(BF)
+
+            w = pltpu.make_async_copy(xx.at[pl.ds(0, 512), pl.ds(q * 512, 512)], out.at[0, :, pl.ds(q * 512, 512)], lsem.at[q])
             w.start()
             written.append(w)
         for w in written:
@@ -371,7 +407,9 @@
     for what, it, _ in steps:
         if what == "send":
             arrived(it.deps)
-            ref = bufs[it.part].at[where(it.spec, "z"), where(it.spec, "y"), where(it.spec, "x"), pl.ds(*it.rows)]
+            kind, blocks, _ = PARTS[it.part]
+            b, at = home[it.part]
+            ref = bufs[b].at[where(it.spec, "z"), where(it.spec, "y"), where(it.spec, "x"), pl.ds(*it.rows), pl.ds(at, max(blocks, 1) * 128)]
             c = pltpu.make_async_remote_copy(
                 src_ref=ref,
                 dst_ref=ref,
@@ -397,38 +435,18 @@
         c.wait_send()
 
 
-def placed_row(values, width):
-    at = lax.rem(lax.axis_index("fs") * width, 128)
-    row = lax.dynamic_update_slice(jnp.zeros((256,), F32), values, (at,))
-    return row[:128] + row[128:]
-
-
 def local(
     tokens, mix_gain, out_gate_w, in_gate_w, value_w, out_gate_scale, in_gate_scale, value_scale, mix_taps, conv_gain,
     out_proj_w, proj_scale, ffn_gain, gate_w, up_w, gate_scale, up_scale, gate_taps, up_taps, gate_bias, up_bias, down_w, down_scale,
 ):
-    pieces = []
-    for c in range(4):
-        pieces += [w[:, c * 128 : c * 128 + 128] for w in (out_gate_w, in_gate_w, value_w)]
-    pieces.append((out_proj_w * proj_scale).T)
-    for j in range(11):
-        pieces += [w[:, j * 128 : j * 128 + 128] for w in (gate_w, up_w)]
-    pieces.append((down_w * down_scale).T)
-    own = jnp.concatenate([p.astype(BF) for p in pieces], axis=1)
-    rows = [placed_row(v, 16) for v in (out_gate_scale, in_gate_scale, value_scale)]
-    rows += [placed_row(v, 44) for v in (gate_scale, up_scale)] + [jnp.zeros((128,), F32)] * 3
-    sown = jnp.stack(rows)
     n = len(PARTS)
     hbm, vmem = pl.BlockSpec(memory_space=pl.ANY), pl.BlockSpec(memory_space=pltpu.VMEM)
-    bufs = [
-        pltpu.VMEM((2, 4, 4, 8, 128), F32) if kind == "s" else pltpu.VMEM((2, 4, 4, 64, blocks * 128), BF)
-        for kind, blocks, _ in PARTS
-    ]
+    bufs = [pltpu.VMEM((2, 4, 4, 64, w), BF) if w else pltpu.VMEM((2, 4, 4, 8, 128), F32) for w in homes()[1]]
     dma = pltpu.SemaphoreType.DMA
     return pl.pallas_call(
         kernel,
         out_shape=jax.ShapeDtypeStruct((1, 512, 2048), BF),
-        in_specs=[hbm, hbm, hbm] + [vmem] * 8,
+        in_specs=[hbm] * 8 + [vmem] * 15,
         out_specs=hbm,
         scratch_shapes=bufs
         + [
@@ -443,16 +461,20 @@
             pltpu.VMEM((1024, 2048), F32),
             pltpu.VMEM((512, 2048), BF),
             pltpu.VMEM((8, 1408), F32),
+            pltpu.VMEM((64, 6272), F32),
+            pltpu.VMEM((16, 128), F32),
             dma((n, 5, 2)),
             dma((n, 5, 2)),
-            dma((n + 1,)),
             dma((8,)),
-            dma((8,)),
+            dma((10,)),
+            dma((10,)),
         ],
         compiler_params=pltpu.CompilerParams(collective_id=0, has_side_effects=True, vmem_limit_bytes=67043328),
         name="layer",
     )(
-        tokens, own, sown, mix_gain[None], mix_taps, conv_gain[None], ffn_gain[None],
+        tokens, out_gate_w, in_gate_w, value_w, out_proj_w.T, gate_w, up_w, down_w.T,
+        out_gate_scale[None], in_gate_scale[None], value_scale[None], gate_scale[None], up_scale[None],
+        proj_scale[None], down_scale[None], mix_gain[None], mix_taps, conv_gain[None], ffn_gain[None],
         gate_taps, up_taps, gate_bias[None], up_bias[None],
     )
 

time: 180 us -> 136 us (0.76)
  local copies, waits for them, and re-layouts: 31.4 us -> 5.75 us
  Pallas kernels: 142 us -> 130 us
  other arithmetic: 6.25 us -> 0 us
    unnamed x43 -> x1, local copies, waits for them, and re-layouts: 23.8 us -> 3.16 us
    pallas_call x1, Pallas kernels: 142 us -> 130 us  [local(): pl.pallas_call(kernel, out_shape=jax.ShapeDtypeStruct((1, 512, 2048), BF)...]
    another operation x8 -> x0, other arithmetic: 4.78 us -> none
    dynamic_update_slice x5 -> x0, local copies, waits for them, and re-layouts: 4.37 us -> none  [placed_row(): row = lax.dynamic_update_slice(jnp.zeros((256,), F32), values, (at,))]
where the time goes in v2:
time: 136 us
  Pallas kernels  130 us (96%)
  local copies, waits for them, and re-layouts  5.75 us (4%)
    pallas_call x1, Pallas kernels, local(): pl.pallas_call(kernel, out_shape=jax.ShapeDtypeStruct((1, 512, 2048), BF)...  130 us
    unnamed x1, local copies, waits for them, and re-layouts  3.16 us

profile of v2, /device:TPU:1, one launch (start us, length us, event | category | flops | bytes accessed | tf_op | source)
XLA Modules:
  0.0 135.8 jit_solution(15631995894400041969)
XLA Ops:
  0.0 1.3 broadcast_in_dim.46.refs_21_
  1.3 1.3 broadcast_in_dim.47.refs_22_
  2.6 130.1 %layer.1 = bf16[1,512,2048]{2,1,0:T(8,128)(2,1)} custom-call(bf16[1,512,2048]{2,1,0:T(8,128)(2,1)} %refs_0_.1, f32[64,512]{1,0:T(8,128)} %refs_1_.1, f32[64,512]{1,0:T(8,128)} %refs_2_.1, f32[64,512]{1,0:T(8,128)} %refs_3_.1, f32[64,512]{1,0:T(8,128)} %bitcast.13, f32[64,1408]{1,0:T(8,128)} %refs_5_.1, f32[64,1408]{1,0:T(8,128)} %refs_6_.1, ...), custom_call_target="tpu_custom_call" | custom-call | tf_op jit(solution)/shard_map/layer/pallas_call | solution.py:446
  132.7 3.2 %copy.25 = bf16[1,512,2048]{2,1,0:T(8,128)(2,1)} copy(bf16[1,512,2048]{2,1,0:T(8,128)(2,1)} %layer.1) | data formatting | bytes 4194304

commit v3 on v2

--- a/solution.py
+++ b/solution.py
@@ -15,19 +15,20 @@
     ("s", 0, "xyz"),
     ("m", 3, "yxz"),
     ("m", 3, "xyz"),
-    ("m", 3, "yxz"),
-    ("m", 3, "zyx"),
-    ("o", 4, "xyz"),
-    ("g", 4, "yzx"),
-    ("g", 2, "yxz"),
-    ("g", 2, "yxz"),
-    ("g", 6, "xzy"),
-    ("g", 4, "zyx"),
+    ("m", 3, "xzy"),
+    ("m", 3, "xzy"),
+    ("o", 4, "yxz"),
+    ("g", 2, "zyx"),
+    ("g", 2, "yzx"),
     ("g", 4, "xyz"),
-    ("d", 4, "xzy"),
-    ("d", 2, "yzx"),
-    ("d", 3, "xzy"),
-    ("d", 2, "yzx"),
+    ("g", 4, "xyz"),
+    ("g", 6, "yzx"),
+    ("g", 2, "xyz"),
+    ("g", 2, "zxy"),
+    ("d", 2, "xyz"),
+    ("d", 2, "xzy"),
+    ("d", 4, "zyx"),
+    ("d", 3, "yzx"),
 )
 
 
@@ -71,20 +72,29 @@
     return made, before
 
 
-def plan(segments, backlog=5.0, latency=2.4, issue=0.06, start=2.0):
+def plan(segments, backlog=5.0, spare=2.0, window=1, latency=2.6, issue=0.12, start=9.0, slower=1.2):
     todo, ends = [], []
     for p, (kind, blocks, order) in enumerate(PARTS):
         made, end = copies_of(p, kind, blocks, order)
+        for op in made:
+            if op.stage == 0 and kind in "ogd":
+                op.deps.append(("cast", kind))
         todo += made
         ends.append(end)
     arrive, link = {}, {(a, s): 0.0 for a in "xyz" for s in (1, -1)}
     out, now, seg = [], start, 0
     while todo or seg < len(segments):
-        moved = True
+        moved, ready = True, False
+        if seg < len(segments):
+            name, us, needs = segments[seg]
+            us *= slower
+            ready = all(arrive.get(k, 1e9) <= now for p in needs for k in ends[p])
         while moved:
             moved = False
+            front = min((op.part for op in todo), default=0)
             for op in todo:
-                if all(arrive.get(d, 1e9) <= now for d in op.deps) and link[op.axis, op.sign] - now < backlog:
+                limit = (backlog if op.part - front < window else spare) + (us if ready else 0.0)
+                if all(arrive.get(d, 1e9) <= now for d in op.deps) and link[op.axis, op.sign] - now < limit:
                     link[op.axis, op.sign] = max(now, link[op.axis, op.sign]) + op.nbytes / RATE
                     arrive[op.key] = link[op.axis, op.sign] + latency
                     out.append(("send", op, now))
@@ -92,15 +102,14 @@
                     todo.remove(op)
                     moved = True
                     break
-        if seg < len(segments):
-            name, us, needs = segments[seg]
-            if all(arrive.get(k, 1e9) <= now for p in needs for k in ends[p]):
-                out.append(("run", segments[seg], now))
-                now += us
-                seg += 1
-                continue
+        if ready:
+            out.append(("run", segments[seg], now))
+            now += us
+            arrive[name] = now
+            seg += 1
+            continue
         later = [v for v in arrive.values() if v > now]
-        later += [v - backlog + 1e-6 for v in link.values() if v - backlog + 1e-6 > now]
+        later += [v - b + 1e-6 for v in link.values() for b in (backlog, spare) if v - b + 1e-6 > now]
         if not later:
             break
         now = min(later)
@@ -124,11 +133,11 @@
 
 
 def segments_of():
-    out = [("norm", 2.4, [])]
+    out = [(("cast", k), 0.4, []) for k in "ogd"] + [(("norm", h), 0.6, []) for h in range(4)]
     m = parts_of("m")
     for c in range(2):
         out.append((("m", c, m[2 * c]), 3.3, m[2 * c : 2 * c + 2] + parts_of("s")))
-    out += [(("o",), 2.4, parts_of("o"))]
+    out += [(("o", q), 0.6, parts_of("o")) for q in range(4)]
     out += [(("f", i), 1.1 if i else 2.8, []) for i in range(4)]
     j = 0
     for p in parts_of("g"):
@@ -138,9 +147,9 @@
     d = parts_of("d")
     k = 0
     for i, p in enumerate(d[:-1]):
-        out += [(("d", p, k, i == 0), PARTS[p][1] * 0.57, [p])]
+        out += [(("d", p, k, i == 0, q), 0.25 + PARTS[p][1] * 0.08, [p]) for q in range(4)]
         k += PARTS[p][1] * 128
-    out += [(("e", d[-1], k), 5.5 + PARTS[d[-1]][1] * 0.6, d[-1:])]
+    out += [(("e", d[-1], k), 6.0 + PARTS[d[-1]][1] * 0.4, d[-1:])]
     return out
 
 
@@ -162,7 +171,7 @@
     home, wide = homes()
     nb = len(wide)
     bufs = refs[24 : 24 + nb]
-    (tt, xx, cc, ss, ssr, ps, pr, hh, yy, dr, sc, wf, sf, ssem, rsem, lsem, tsem, trsem) = refs[24 + nb :]
+    (tt, xx, cc, ss, ssr, ps, pr, hh, yy, sc, wf, sf, credit, ssem, rsem, lsem, tsem, trsem) = refs[24 + nb :]
     rep, fs, tp = lax.axis_index("rep"), lax.axis_index("fs"), lax.axis_index("tp")
     z, y, x = fs // 16, lax.rem(fs // 4, 4), lax.rem(fs, 4)
     pos = dict(x=x, y=y, z=z)
@@ -192,14 +201,9 @@
             pl.semaphore_signal(barrier, inc=1, device_id=beside(axis, sign), device_id_type=MESH)
     pl.semaphore_signal(barrier, inc=1, device_id=mate, device_id_type=MESH)
 
-    for c in local[:-1]:
-        c.wait()
-    eye = lax.broadcasted_iota(jnp.int32, (64, 64), 0) == lax.broadcasted_iota(jnp.int32, (64, 64), 1)
-    p_col, d_col = (jnp.sum(jnp.where(eye, v[...], 0.0), axis=1, keepdims=True) for v in (s_p, s_d))
-    last = {}
-    for p, (kind, blocks, _) in enumerate(PARTS):
-        first = last.get(kind, 0)
-        last[kind] = first + blocks
+    def cast(kind):
+        for i in dict(m=(0, 1, 2), o=(3,), g=(4, 5), d=(6,), s=())[kind]:
+            local[i].wait()
         if kind == "s":
             sf[...] = jnp.zeros((16, 128), F32)
             for k, v in enumerate((s_o, s_i, s_v)):
@@ -208,20 +212,27 @@
                 sf[11 + k : 12 + k, 0:44] = v[...]
             low = pltpu.roll(sf[0:8, :], lax.rem(fs * 16, 128), 1)
             high = pltpu.roll(sf[8:16, :], lax.rem(fs * 44, 128), 1)
-            bufs[home[p][0]][z, y, x] = low + high
-            continue
-        for b in range(blocks):
-            j = first + b
-            if kind == "m":
-                v = wf[:, pl.ds((j % 3) * 512 + j // 3 * 128, 128)]
-            elif kind == "o":
-                v = wf[:, pl.ds(1536 + j * 128, 128)] * p_col
-            elif kind == "g":
-                v = wf[:, pl.ds(2048 + (j % 2) * 1408 + j // 2 * 128, 128)]
-            else:
-                v = wf[:, pl.ds(2048 + 2816 + j * 128, 128)] * d_col
-            at = home[p][1] + b * 128
-            bufs[home[p][0]][z, y, x, :, at : at + 128] = v.astype(BF)
+            bufs[home[parts_of("s")[0]][0]][z, y, x] = low + high
+            return
+        column = None
+        if kind in "od":
+            eye = lax.broadcasted_iota(jnp.int32, (64, 64), 0) == lax.broadcasted_iota(jnp.int32, (64, 64), 1)
+            column = jnp.sum(jnp.where(eye, (s_p if kind == "o" else s_d)[...], 0.0), axis=1, keepdims=True)
+        j = 0
+        for p in parts_of(kind):
+            for b in range(PARTS[p][1]):
+                if kind == "m":
+                    v = wf[:, pl.ds((j % 3) * 512 + j // 3 * 128, 128)]
+                elif kind == "g":
+                    v = wf[:, pl.ds(2048 + (j % 2) * 1408 + j // 2 * 128, 128)]
+                else:
+                    v = wf[:, pl.ds((1536 if kind == "o" else 2048 + 2816) + j * 128, 128)] * column
+                at = home[p][1] + b * 128
+                bufs[home[p][0]][z, y, x, :, at : at + 128] = v.astype(BF)
+                j += 1
+
+    cast("s")
+    cast("m")
     pl.semaphore_wait(barrier, 7)
 
     def to_mate(src, dst, k):
@@ -231,7 +242,6 @@
 
     tokens_over = to_mate(tok.at[0], tt.at[pl.ds(mine, 512)], 0)
     tokens_over.start()
-    local[-1].wait()
 
     def where(spec, axis):
         v = spec[axis]
@@ -247,10 +257,12 @@
     def whole(p, cols):
         return bufs[home[p][0]][:, :, :, :, cols].reshape(2048, -1)
 
-    def run_norm():
-        tokens_over.wait()
-
-        @pl.loop(0, 1024 // 64)
+    def run_norm(h):
+        if h == 0:
+            local[-1].wait()
+            tokens_over.wait()
+
+        @pl.loop(h * 4, h * 4 + 4)
         def _(i):
             r = rows_of(i, 64)
             v = tt[r, :].astype(F32)
@@ -310,14 +322,15 @@
     def eighths(p, q):
         return bufs[home[p][0]][q // 2, pl.ds(q % 2 * 2, 2)].reshape(512, -1)
 
-    def run_o():
+    def run_o(q):
         (p,) = parts_of("o")
-        squares_over.start()
-        for q in range(4):
-            ps[:, q * 512 : q * 512 + 512] = dot_nt(cc[...], eighths(p, q)).astype(BF)
-            if q:
-                p_over(q - 1).start()
-        p_over(3).start()
+        if q == 0:
+            squares_over.start()
+        ps[:, q * 512 : q * 512 + 512] = dot_nt(cc[...], eighths(p, q)).astype(BF)
+        if q:
+            p_over(q - 1).start()
+        if q == 3:
+            p_over(3).start()
 
     def run_f(i):
         if i == 0:
@@ -336,9 +349,12 @@
             v = v * lax.rsqrt(jnp.mean(v * v, axis=1, keepdims=True) + EPS) * fgain[...]
             xx[r, :] = v.astype(BF)
 
+        if i == 3:
+            pl.semaphore_signal(credit, inc=1, device_id=mate, device_id_type=MESH)
+
     def run_g(j, p, b):
         cols = slice(j * 128, j * 128 + 128)
-        tg, tu, bg, bu = gtaps[:, cols], utaps[:, cols], gbias[:, cols], ubias[:, cols]
+        tg, tu, bg, bu = gtaps[:, cols], utaps[:, cols], gbias[cols][None], ubias[cols][None]
         sg, su = sc[3:4, cols], sc[4:5, cols]
 
         tg, tu = tg * sg, tu * su
@@ -355,16 +371,15 @@
         zero = jnp.zeros((8, 128), F32)
         lax.fori_loop(0, 1024 // TM, tile, (zero, zero))
 
-    def run_d(p, k, first):
-        for q in range(4):
-            w = eighths(p, q)
-            v = dot_nt(hh[:, k : k + w.shape[1]], w)
-            c = slice(q * 512, q * 512 + 512)
-            yy[0:1024, c] = v if first else yy[0:1024, c] + v
+    def run_d(p, k, first, q):
+        w = eighths(p, q)
+        v = dot_nt(hh[:, k : k + w.shape[1]], w)
+        c = slice(q * 512, q * 512 + 512)
+        yy[:, c] = v if first else yy[:, c] + v
 
     def d_over(q):
         c = pl.ds(q * 512, 512)
-        return to_mate(ps.at[pl.ds(0, 512), c], dr.at[:, c], 6 + q)
+        return to_mate(ps.at[pl.ds(0, 512), c], pr.at[pl.ds(0, 512), c], 6 + q)
 
     def run_e(p, k):
         own, far = pl.ds(mine, 512), pl.ds(other, 512)
@@ -372,10 +387,11 @@
             w = eighths(p, q)
             c = slice(q * 512, q * 512 + 512)
             ps[0:512, c] = (yy[far, c] + dot_nt(hh[far, k : k + w.shape[1]], w)).astype(BF)
+            if q == 1:
+                pl.semaphore_wait(credit, 1)
             if q:
                 d_over(q - 1).start()
         d_over(3).start()
-        written = []
         for q in range(4):
             w = eighths(p, q)
             c = slice(q * 512, q * 512 + 512)
@@ -386,20 +402,14 @@
             def _(i):
                 r = pl.ds(pl.multiple_of(mine + i * 64, 64), 64)
                 o = rows_of(i, 64)
-                xx[o, c] = (tt[r, c].astype(F32) + yy[r, c] + dr[o, c].astype(F32)).astype(BF)
-
-            w = pltpu.make_async_copy(xx.at[pl.ds(0, 512), pl.ds(q * 512, 512)], out.at[0, :, pl.ds(q * 512, 512)], lsem.at[q])
-            w.start()
-            written.append(w)
-        for w in written:
-            w.wait()
+                out[0, o, c] = (tt[r, c].astype(F32) + yy[r, c] + pr[o, c].astype(F32)).astype(BF)
 
     steps, ends = plan(segments_of())
     started, got = {}, set()
 
     def arrived(keys):
         for key in keys:
-            if key not in got:
+            if key not in got and key[0] != "cast":
                 got.add(key)
                 started[key].wait_recv()
 
@@ -424,13 +434,10 @@
         name, _, needs = it
         for p in needs:
             arrived(ends[p])
-        if name == "norm":
-            run_norm()
-            continue
         if name[0] == "m" and not scaled:
             scaled = True
             run_scales(parts_of("s")[0])
-        dict(m=run_m, o=run_o, f=run_f, g=run_g, d=run_d, e=run_e)[name[0]](*name[1:])
+        dict(cast=cast, norm=run_norm, m=run_m, o=run_o, f=run_f, g=run_g, d=run_d, e=run_e)[name[0]](*name[1:])
     for c in started.values():
         c.wait_send()
 
@@ -445,9 +452,9 @@
     dma = pltpu.SemaphoreType.DMA
     return pl.pallas_call(
         kernel,
-        out_shape=jax.ShapeDtypeStruct((1, 512, 2048), BF),
+        out_shape=pltpu.VMEM((1, 512, 2048), BF),
         in_specs=[hbm] * 8 + [vmem] * 15,
-        out_specs=hbm,
+        out_specs=vmem,
         scratch_shapes=bufs
         + [
             pltpu.VMEM((1024, 2048), BF),
@@ -459,23 +466,23 @@
             pltpu.VMEM((1024, 2048), BF),
             pltpu.VMEM((1024, 1408), BF),
             pltpu.VMEM((1024, 2048), F32),
-            pltpu.VMEM((512, 2048), BF),
             pltpu.VMEM((8, 1408), F32),
             pltpu.VMEM((64, 6272), F32),
             pltpu.VMEM((16, 128), F32),
+            pltpu.SemaphoreType.REGULAR,
             dma((n, 5, 2)),
             dma((n, 5, 2)),
             dma((8,)),
             dma((10,)),
             dma((10,)),
         ],
-        compiler_params=pltpu.CompilerParams(collective_id=0, has_side_effects=True, vmem_limit_bytes=67043328),
+        compiler_params=pltpu.CompilerParams(collective_id=0, has_side_effects=True, vmem_limit_bytes=64600000),
         name="layer",
     )(
         tokens, out_gate_w, in_gate_w, value_w, out_proj_w.T, gate_w, up_w, down_w.T,
         out_gate_scale[None], in_gate_scale[None], value_scale[None], gate_scale[None], up_scale[None],
         proj_scale[None], down_scale[None], mix_gain[None], mix_taps, conv_gain[None], ffn_gain[None],
-        gate_taps, up_taps, gate_bias[None], up_bias[None],
+        gate_taps, up_taps, gate_bias, up_bias,
     )
 
 

time: 136 us -> 130 us (0.956)
  local copies, waits for them, and re-layouts: 5.75 us -> 1.32 us
  Pallas kernels: 130 us -> 128 us
    broadcast_in_dim x2 -> x0, local copies, waits for them, and re-layouts: 2.59 us -> none  [the longest x1 1.29 us: local(): up_bias[None]]
    unnamed x1, local copies, waits for them, and re-layouts: 3.16 us -> 1.32 us
    pallas_call x1, Pallas kernels: 130 us -> 128 us  [local(): pl.pallas_call(kernel, out_shape=pltpu.VMEM((1, 512, 2048), BF), in_specs...]
where the time goes in v3:
time: 130 us
  Pallas kernels  128 us (98%)
  local copies, waits for them, and re-layouts  1.32 us (1%)
    pallas_call x1, Pallas kernels, local(): pl.pallas_call(kernel, out_shape=pltpu.VMEM((1, 512, 2048), BF), in_specs...  128 us

profile of v3, /device:TPU:1, one launch (start us, length us, event | category | flops | bytes accessed | tf_op | source)
XLA Modules:
  0.0 129.6 jit_solution(11392493545111922642)
XLA Ops:
  0.0 128.3 %layer.1 = bf16[1,512,2048]{2,1,0:T(8,128)(2,1)S(1)} custom-call(bf16[1,512,2048]{2,1,0:T(8,128)(2,1)} %refs_0_.1, f32[64,512]{1,0:T(8,128)} %refs_1_.1, f32[64,512]{1,0:T(8,128)} %refs_2_.1, f32[64,512]{1,0:T(8,128)} %refs_3_.1, f32[64,512]{1,0:T(8,128)} %bitcast.13, f32[64,1408]{1,0:T(8,128)} %refs_5_.1, f32[64,1408]{1,0:T(8,128)} %refs_6_.1, ...), custom_call_target="tpu_custom_call" | custom-call | tf_op jit(solution)/shard_map/layer/pallas_call | solution.py:453
  128.3 1.3 %copy.25 = bf16[1,512,2048]{2,1,0:T(8,128)(2,1)} copy(bf16[1,512,2048]{2,1,0:T(8,128)(2,1)S(1)} %layer.1) | data formatting | bytes 4194304
